TPU v7x, 32 devices: a whole 2x2x4 slice. The times are simulated.
32 devices in a mesh: ep: 8 (over z, core), tp: 4 (over y, x).
Axes of the slice: x: 2, y: 2, z: 4, core: 2. Of those that a mesh axis runs over, the one named last changes fastest.
Arguments:
- tokens: bfloat16 [1536, 2048], P('ep'), may hold values from -6 to 6
- moe_out: bfloat16 [1536, 2048], P('ep', 'tp'), may hold values from -16 to 16
- out_grad: bfloat16 [1536, 2048], P('ep', 'tp'), may hold values from -3 to 3
- norm_gain: float32 [2048], P('tp'), may hold values from 0.1 to 1.9
- gate_weights: bfloat16 [1536, 2], P('ep'), may hold values from 0.099609375 to 1
- expert_ids: int32 [1536, 2], P('ep'), may hold values from 0 to 7, as said below
- gate_w: bfloat16 [8, 1536, 2048], P('ep', 'tp'), may hold values from -0.125 to 0.125
- up_w: bfloat16 [8, 1536, 2048], P('ep', 'tp'), may hold values from -0.125 to 0.125
- down_w: bfloat16 [8, 1536, 2048], P('ep', 'tp'), may hold values from -0.15625 to 0.15625
Outputs:
- token_grad: bfloat16 [1536, 2048], P('ep', 'tp')
- gate_grad: bfloat16 [1536, 2], P('ep')
- gate_w_grad: float32 [8, 1536, 2048], P('ep', 'tp')
- up_w_grad: float32 [8, 1536, 2048], P('ep', 'tp')
- down_w_grad: float32 [8, 1536, 2048], P('ep', 'tp')
Inputs may be any that keep to these rules, and one draw needn't show every extreme that they name: `expert_ids`: each row names 2 different experts of one group, ids g * 2 to g * 2 + 1. In each aligned block of 192 rows (the rows of one device) no expert is named more than 96 times, and in every draw all experts of one group are named exactly 96 times in every block.
All inputs are finite; a program needn't handle non-finite values.
Results may differ from a plain program's by a relative error of at most 0.015.
Values may be sent and summed in bfloat16 or wider, within the bound.
A program may use at most 64 MiB of HBM per device.

v0:
```python
import jax
import jax.numpy as jnp
from jax import lax
from jax.sharding import PartitionSpec as P

EPSILON = 0.25


def pick_rows(matrix, slot_token, n_experts, capacity):
    padded = jnp.concatenate([matrix, jnp.zeros((1, matrix.shape[1]), matrix.dtype)], axis=0)
    return padded[slot_token].reshape(n_experts, capacity, matrix.shape[1])


def local(tokens, moe_out, out_grad, norm_gain, gate_weights, expert_ids, gate_w, up_w, down_w):
    tok_count = tokens.shape[0]
    full_width = tokens.shape[1]
    col_width = moe_out.shape[1]
    ep_count = lax.axis_size("ep")
    exp_local = gate_w.shape[0]
    n_experts = ep_count * exp_local
    top_count = expert_ids.shape[1]
    capacity = 2 * tok_count * top_count // n_experts
    mixed = moe_out.astype(jnp.float32)
    scaled_grad = out_grad.astype(jnp.float32) * norm_gain
    squares, crossed = lax.psum(
        (jnp.sum(mixed * mixed, axis=1), jnp.sum(scaled_grad * mixed, axis=1)), "tp"
    )
    inverse = lax.rsqrt(squares / full_width + EPSILON)
    coupling = inverse**3 * (crossed / full_width)
    mix_grad = (inverse[:, None] * scaled_grad - mixed * coupling[:, None]).astype(jnp.bfloat16)
    assigned = expert_ids.reshape(-1)
    n_assign = assigned.shape[0]
    one_hot = (assigned[:, None] == jnp.arange(n_experts, dtype=jnp.int32)[None, :]).astype(
        jnp.int32
    )
    before = jnp.sum((jnp.cumsum(one_hot, axis=0) - one_hot) * one_hot, axis=1)
    slot_of = assigned * capacity + before
    slot_source = (
        jnp.full((n_experts * capacity,), n_assign, jnp.int32)
        .at[slot_of]
        .set(jnp.arange(n_assign, dtype=jnp.int32))
    )
    slot_token = slot_source // top_count
    weight_pad = jnp.concatenate([gate_weights.reshape(-1), jnp.zeros((1,), jnp.bfloat16)])
    send_weight = weight_pad[slot_source].reshape(n_experts, capacity)
    token_slice = lax.dynamic_slice_in_dim(tokens, lax.axis_index("tp") * col_width, col_width, 1)
    part_tokens, part_grad, recv_weight = (
        lax.all_to_all(
            pick_rows(token_slice, slot_token, n_experts, capacity),
            "ep",
            split_axis=0,
            concat_axis=0,
            tiled=True,
        ),
        lax.all_to_all(
            pick_rows(mix_grad, slot_token, n_experts, capacity),
            "ep",
            split_axis=0,
            concat_axis=0,
            tiled=True,
        ),
        lax.all_to_all(send_weight, "ep", split_axis=0, concat_axis=0, tiled=True),
    )
    recv_tokens, recv_grad = (
        lax.all_gather(part_tokens, "tp", axis=2, tiled=True),
        lax.all_gather(part_grad, "tp", axis=2, tiled=True),
    )
    layout = (ep_count, exp_local, capacity, full_width)
    inputs = recv_tokens.reshape(layout)
    cotangent = recv_grad.reshape(layout)
    scales = recv_weight.reshape(ep_count, exp_local, capacity, 1).astype(jnp.float32)
    gate_pre = jnp.einsum("secd,efd->secf", inputs, gate_w, preferred_element_type=jnp.float32)
    up_pre = jnp.einsum("secd,efd->secf", inputs, up_w, preferred_element_type=jnp.float32)
    hidden_grad = jnp.einsum(
        "secd,efd->secf", cotangent, down_w, preferred_element_type=jnp.float32
    )
    sigmoid = jax.nn.sigmoid(gate_pre)
    activated = gate_pre * sigmoid
    gate_part = jnp.sum(activated * up_pre * hidden_grad, axis=3)
    scaled_hidden = (scales * activated * up_pre).astype(jnp.bfloat16)
    down_grad = jnp.einsum(
        "secf,secd->efd", scaled_hidden, cotangent, preferred_element_type=jnp.float32
    )
    gate_delta = (
        scales * hidden_grad * up_pre * sigmoid * (1.0 + gate_pre * (1.0 - sigmoid))
    ).astype(jnp.bfloat16)
    up_delta = (scales * hidden_grad * activated).astype(jnp.bfloat16)
    gate_grad_w = jnp.einsum(
        "secf,secd->efd", gate_delta, inputs, preferred_element_type=jnp.float32
    )
    up_grad_w = jnp.einsum("secf,secd->efd", up_delta, inputs, preferred_element_type=jnp.float32)
    partial_value = jnp.einsum(
        "secf,efd->secd", gate_delta, gate_w, preferred_element_type=jnp.float32
    )
    partial_value = partial_value + jnp.einsum(
        "secf,efd->secd", up_delta, up_w, preferred_element_type=jnp.float32
    )
    gate_total = lax.psum(gate_part, "tp").astype(jnp.bfloat16)
    slot_grad = lax.psum_scatter(
        partial_value.astype(jnp.bfloat16), "tp", scatter_dimension=3, tiled=True
    )
    back_grad, back_gate = (
        lax.all_to_all(
            slot_grad.reshape(ep_count * exp_local, capacity, col_width),
            "ep",
            split_axis=0,
            concat_axis=0,
            tiled=True,
        ),
        lax.all_to_all(
            gate_total.reshape(ep_count * exp_local, capacity),
            "ep",
            split_axis=0,
            concat_axis=0,
            tiled=True,
        ),
    )
    token_rows = back_grad.reshape(n_experts * capacity, col_width)[slot_of].reshape(
        tok_count, top_count, col_width
    )
    token_grad = jnp.sum(token_rows.astype(jnp.float32), axis=1).astype(jnp.bfloat16)
    gate_grad = back_gate.reshape(-1)[slot_of].reshape(tok_count, top_count)
    return (token_grad, gate_grad, gate_grad_w, up_grad_w, down_grad)


def solution(mesh):
    in_specs = (
        P("ep", None),
        P("ep", "tp"),
        P("ep", "tp"),
        P("tp"),
        P("ep", None),
        P("ep", None),
        P("ep", "tp", None),
        P("ep", "tp", None),
        P("ep", "tp", None),
    )
    out_specs = (
        P("ep", "tp"),
        P("ep", None),
        P("ep", "tp", None),
        P("ep", "tp", None),
        P("ep", "tp", None),
    )
    return jax.shard_map(local, mesh=mesh, in_specs=in_specs, out_specs=out_specs, check_vma=False)
```

profile of v0, /device:TPU:0, one launch (start us, length us, event | category | flops | bytes accessed | tf_op | source)
XLA Modules:
  0.0 224.4 jit_solution(5466706563891918215)
XLA Ops:
  10.6 2.9 %scatter_custom_fusion = s32[768]{0:T(1024)S(1)} fusion(s32[384]{0:T(512)S(1)} %fusion.37, s32[384]{0:T(512)S(1)} %iota.11, s32[]{:T(128)} %constant.18.clone.1), kind=kCustom, calls=%fused_computation.62 | custom fusion | bytes 3076 | tf_op jit(solution)/shard_map/scatter | solution.py:41
  14.6 2.7 %gather_fusion.2 = bf16[768,512]{1,0:T(8,128)(2,1)S(1)} fusion(bf16[193,512]{1,0:T(8,128)(2,1)S(1)} %concatenate.11, s32[1024]{0:T(1024)S(1)} %get-tuple-element.31), kind=kCustom, calls=%fused_computation.2 | custom fusion | bytes 1575936 | tf_op jit(solution)/shard_map/gather | solution.py:11
  17.3 27.3 %all_to_all.31 = bf16[8,96,512]{2,1,0:T(8,128)(2,1)} all-to-all(bf16[8,96,512]{2,1,0:T(8,128)(2,1)S(1)} %bitcast.94), channel_id=1, replica_groups=mesh['ep'=8,'tp'=4] {'ep'}, dimensions={0} | all-to-all | bytes 1572864 | tf_op jit(solution)/shard_map/all_to_all | solution.py:48
  44.9 10.0 %all-reduce.2 = (f32[192]{0:T(256)S(1)}, f32[192]{0:T(256)S(1)}) all-reduce(f32[192]{0:T(256)S(1)} %get-tuple-element.21, f32[192]{0:T(256)S(1)} %get-tuple-element.20), channel_id=1, replica_groups=mesh['ep'=8,'tp'=4] {'tp'}, use_global_device_ids=true, to_apply=%region_7.8 | all-reduce | flops 384 | bytes 3072 | tf_op jit(solution)/shard_map/psum | solution.py:25
  55.1 2.7 %gather_fusion.1 = bf16[768,512]{1,0:T(8,128)(2,1)S(1)} fusion(bf16[193,512]{1,0:T(8,128)(2,1)S(1)} %concatenate.10, s32[1024]{0:T(1024)S(1)} %get-tuple-element.31), kind=kCustom, calls=%fused_computation.1 | custom fusion | bytes 1575936 | tf_op jit(solution)/shard_map/gather | solution.py:11
  57.8 24.0 %all_to_all.32 = bf16[8,96,512]{2,1,0:T(8,128)(2,1)} all-to-all(bf16[8,96,512]{2,1,0:T(8,128)(2,1)S(1)} %bitcast.93), channel_id=1, replica_groups=mesh['ep'=8,'tp'=4] {'ep'}, dimensions={0} | all-to-all | bytes 1572864 | tf_op jit(solution)/shard_map/all_to_all | solution.py:55
  82.3 5.0 %gather_fusion = bf16[768]{0:T(1024)(128)(2,1)S(1)} fusion(bf16[385]{0:T(512)(128)(2,1)S(1)} %pad_maximum_fusion, s32[1024]{0:T(1024)S(1)} %get-tuple-element.32), kind=kCustom, calls=%fused_computation | custom fusion | bytes 6144 | tf_op jit(solution)/shard_map/gather | solution.py:45
  87.3 7.9 %all_to_all.33 = bf16[8,1,96]{2,1,0:T(2,128)(2,1)S(1)} all-to-all(bf16[8,1,96]{2,1,0:T(2,128)(2,1)S(1)} %all_to_all.25), channel_id=1, replica_groups=mesh['ep'=8,'tp'=4] {'ep'}, dimensions={0} | all-to-all | bytes 3072 | tf_op jit(solution)/shard_map/all_to_all | solution.py:62
  95.3 5.2 %fusion.13 = f32[8,1,96,384]{3,2,0,1:T(8,128)} fusion(bf16[8,96,2048]{2,1,0:T(8,128)(2,1)} %all-gather.5.cloned.1.call-done, bf16[1,384,2048]{2,1,0:T(8,128)(2,1)S(1)} %copy-done.3), kind=kOutput, calls=%fused_computation.21 | convolution fusion | flops 1207959552 | bytes 5898240 | tf_op jit(solution)/shard_map/secd,efd->secf/dot_general | solution.py:73
  100.5 2.9 %fusion.16 = f32[8,1,96,384]{3,2,0,1:T(8,128)} fusion(bf16[8,96,2048]{2,1,0:T(8,128)(2,1)S(1)} %copy-done.1, bf16[1,384,2048]{2,1,0:T(8,128)(2,1)S(1)} %copy-done), kind=kOutput, calls=%fused_computation.22 | convolution fusion | flops 1207959552 | bytes 5898240 | tf_op jit(solution)/shard_map/secd,efd->secf/dot_general | solution.py:72
  103.4 29.6 %all-gather.3.cloned.1.call-done = bf16[8,96,2048]{2,1,0:T(8,128)(2,1)} async-done(((bf16[8,96,512]{2,1,0:T(8,128)(2,1)}), bf16[8,96,2048]{2,1,0:T(8,128)(2,1)}) %all-gather.3.cloned.1.call-update) | async-done | bytes 3145744 | tf_op jit(solution)/shard_map/all_gather | solution.py:66
  133.0 5.3 %multiply_reduce_fusion = (f32[8,96]{1,0:T(8,128)S(1)}, bf16[8,1,96,384]{3,2,0,1:T(8,128)(2,1)S(1)}, bf16[8,96,384]{2,1,0:T(8,128)(2,1)S(1)}) fusion(f32[8,1,96,384]{3,2,0,1:T(8,128)} %fusion.13, f32[8,1,96,384]{3,2,0,1:T(8,128)} %fusion.16, f32[8,96]{1,0:T(8,128)S(1)} %bitcast.97, bf16[8,96,2048]{2,1,0:T(8,128)(2,1)} %all-gather.3.cloned.1.call-done, ...), kind=kOutput, calls=%fused_computation.24 | convolution fusion | flops 1212972288 | bytes 8263680 | tf_op jit(solution)/shard_map/secd,efd->secf/dot_general | solution.py:74
  140.2 3.5 %fusion = bf16[8,1,96,2048]{3,2,0,1:T(8,128)(2,1)} fusion(f32[8,96,2048]{2,1,0:T(8,128)S(1)} %fusion.1, bf16[8,96,384]{2,1,0:T(8,128)(2,1)S(1)} %get-tuple-element.26, bf16[1,384,2048]{2,1,0:T(8,128)(2,1)S(1)} %copy-done.4), kind=kOutput, calls=%fused_computation.7 | convolution fusion | flops 1211105280 | bytes 11599872 | tf_op jit(solution)/shard_map/secf,efd->secd/dot_general | solution.py:95
  143.7 16.7 %psum.23 = bf16[8,1,96]{2,1,0:T(2,128)(2,1)} all-reduce(f32[8,1,96]{2,1,0:T(1,128)S(1)} %bitcast.99), channel_id=1, replica_groups=mesh['ep'=8,'tp'=4] {'tp'}, use_global_device_ids=true, to_apply=%region_11.12 | all-reduce | flops 768 | bytes 4608 | tf_op jit(solution)/shard_map/psum | solution.py:98
  160.4 4.6 %all-to-all-start.4 = ((bf16[8,1,96]{2,1,0:T(2,128)(2,1)}), bf16[8,1,96]{2,1,0:T(2,128)(2,1)S(1)}, u32[]{:S(2)}, u32[]{:S(2)}) async-start(bf16[8,1,96]{2,1,0:T(2,128)(2,1)} %psum.23), calls=%async_computation.5 | async-start | bytes 8192 | tf_op jit(solution)/shard_map/all_to_all | solution.py:110
  165.0 5.5 %all-to-all-done.4 = bf16[8,1,96]{2,1,0:T(2,128)(2,1)S(1)} async-done(((bf16[8,1,96]{2,1,0:T(2,128)(2,1)}), bf16[8,1,96]{2,1,0:T(2,128)(2,1)S(1)}, u32[]{:S(2)}, u32[]{:S(2)}) %all-to-all-start.4) | async-done | bytes 1568 | tf_op jit(solution)/shard_map/all_to_all | solution.py:110
  170.5 17.9 %reduce-scatter.2.cloned.1.call-done = bf16[8,1,96,512]{3,2,0,1:T(8,128)(2,1)} async-done(((bf16[8,1,96,2048]{3,2,0,1:T(8,128)(2,1)}), bf16[8,1,96,512]{3,2,0,1:T(8,128)(2,1)}) %reduce-scatter.2.cloned.1.call-update) | async-done | bytes 786448 | tf_op jit(solution)/shard_map/reduce_scatter | solution.py:99
  188.4 4.6 %all-to-all-start.3 = ((bf16[8,96,512]{2,1,0:T(8,128)(2,1)}), bf16[8,96,512]{2,1,0:T(8,128)(2,1)S(1)}, u32[]{:S(2)}, u32[]{:S(2)}) async-start(bf16[8,96,512]{2,1,0:T(8,128)(2,1)} %bitcast.95), calls=%async_computation.4 | async-start | bytes 1572864 | tf_op jit(solution)/shard_map/all_to_all | solution.py:103
  193.0 5.1 %convolution_bitcast_fusion.1 = f32[1,384,2048]{2,1,0:T(8,128)} fusion(bf16[8,96,384]{2,1,0:T(8,128)(2,1)S(1)} %get-tuple-element.26, bf16[8,96,2048]{2,1,0:T(8,128)(2,1)} %all-gather.5.cloned.1.call-done), kind=kOutput, calls=%fused_computation.9 | convolution fusion | flops 1207959552 | bytes 6881280 | tf_op jit(solution)/shard_map/secf,secd->efd/dot_general | solution.py:91
  198.2 3.1 %convolution_bitcast_fusion.2 = f32[1,384,2048]{2,1,0:T(8,128)} fusion(bf16[8,96,2048]{2,1,0:T(8,128)(2,1)S(1)} %copy-done.2, bf16[8,1,96,384]{3,2,0,1:T(8,128)(2,1)S(1)} %get-tuple-element.25), kind=kOutput, calls=%fused_computation.10 | convolution fusion | flops 1207959552 | bytes 6881280 | tf_op jit(solution)/shard_map/secf,secd->efd/dot_general | solution.py:88
  201.3 3.3 %convolution_bitcast_fusion = f32[1,384,2048]{2,1,0:T(8,128)} fusion(bf16[8,96,2048]{2,1,0:T(8,128)(2,1)S(1)} %copy-done.9, f32[8,1,96,384]{3,2,0,1:T(8,128)S(1)} %copy-done.10, f32[8,96]{1,0:T(8,128)S(1)} %bitcast.98, f32[8,1,96,384]{3,2,0,1:T(8,128)S(1)} %copy-done.11), kind=kOutput, calls=%fused_computation.8 | convolution fusion | flops 1210023936 | bytes 8653824 | tf_op jit(solution)/shard_map/secf,secd->efd/dot_general | solution.py:81
  204.7 2.8 %gather_fusion.4 = bf16[384]{0:T(512)(128)(2,1)S(1)} fusion(bf16[768]{0:T(1024)(128)(2,1)S(1)} %reshape.162, s32[1024]{0:T(1024)S(1)} %pad_clamp_fusion), kind=kCustom, calls=%fused_computation.4 | custom fusion | bytes 3072 | tf_op jit(solution)/shard_map/gather | solution.py:122
  208.3 5.6 %all-to-all-done.3 = bf16[8,96,512]{2,1,0:T(8,128)(2,1)S(1)} async-done(((bf16[8,96,512]{2,1,0:T(8,128)(2,1)}), bf16[8,96,512]{2,1,0:T(8,128)(2,1)S(1)}, u32[]{:S(2)}, u32[]{:S(2)}) %all-to-all-start.3) | async-done | bytes 786464 | tf_op jit(solution)/shard_map/all_to_all | solution.py:103
  214.0 2.1 gather_fusion.3
  (65 shorter events, 9.9 us)
Async XLA Ops:
  7.2 93.4 %copy-start = (bf16[1,384,2048]{2,1,0:T(8,128)(2,1)S(1)}, bf16[1,384,2048]{2,1,0:T(8,128)(2,1)}, u32[]{:S(2)}) copy-start(bf16[1,384,2048]{2,1,0:T(8,128)(2,1)} %param.15) | copy-start | bytes 4718596
  7.2 88.1 %all-gather.5.cloned.1.call-start = ((), (), s32[]{:S(2)}) async-start(), calls=%async_computation.7 | async-start | bytes 3932160 | tf_op jit(solution)/shard_map/all_gather | solution.py:65
  17.3 27.4 %copy-start.5 = (bf16[192,512]{1,0:T(8,128)(2,1)S(1)}, bf16[192,512]{1,0:T(8,128)(2,1)}, u32[]{:S(2)}) copy-start(bf16[192,512]{1,0:T(8,128)(2,1)} %param.10) | copy-start | bytes 589828
  17.3 27.4 %copy-start.6 = (bf16[192,512]{1,0:T(8,128)(2,1)S(1)}, bf16[192,512]{1,0:T(8,128)(2,1)}, u32[]{:S(2)}) copy-start(bf16[192,512]{1,0:T(8,128)(2,1)} %param.11) | copy-start | bytes 589828
  17.3 27.4 %copy-start.7 = (f32[512]{0:T(512)S(1)}, f32[512]{0:T(512)}, u32[]{:S(2)}) copy-start(f32[512]{0:T(512)} %param.12) | copy-start | bytes 6148
  44.7 88.4 %all-gather.3.cloned.1.call-start = ((), (), s32[]{:S(2)}) async-start(), calls=%async_computation.6 | async-start | bytes 3932160 | tf_op jit(solution)/shard_map/all_gather | solution.py:66
  57.8 24.1 %copy-start.8 = (bf16[192,2]{0,1:T(2,128)(2,1)S(1)}, bf16[192,2]{0,1:T(2,128)(2,1)}, u32[]{:S(2)}) copy-start(bf16[192,2]{0,1:T(2,128)(2,1)} %param.13) | copy-start | bytes 2308
  81.8 13.5 %copy-start.3 = (bf16[1,384,2048]{2,1,0:T(8,128)(2,1)S(1)}, bf16[1,384,2048]{2,1,0:T(8,128)(2,1)}, u32[]{:S(2)}) copy-start(bf16[1,384,2048]{2,1,0:T(8,128)(2,1)} %param.16) | copy-start | bytes 4718596
  81.9 106.5 %reduce-scatter.2.cloned.1.call-start = ((), (), s32[]{:S(2)}) async-start(), calls=%async_computation.8 | async-start | bytes 3932160 | tf_op jit(solution)/shard_map/reduce_scatter | solution.py:99
  95.3 5.2 %copy-start.1 = (bf16[8,96,2048]{2,1,0:T(8,128)(2,1)S(1)}, bf16[8,96,2048]{2,1,0:T(8,128)(2,1)}, u32[]{:S(2)}) copy-start(bf16[8,96,2048]{2,1,0:T(8,128)(2,1)} %all-gather.5.cloned.1.call-done) | copy-start | bytes 9437188
  138.4 1.8 copy-start.4
  160.4 10.1 %all-to-all-start.4 = ((bf16[8,1,96]{2,1,0:T(2,128)(2,1)}), bf16[8,1,96]{2,1,0:T(2,128)(2,1)S(1)}, u32[]{:S(2)}, u32[]{:S(2)}) async-start(bf16[8,1,96]{2,1,0:T(2,128)(2,1)} %psum.23), calls=%async_computation.5 | async-start | bytes 8192 | tf_op jit(solution)/shard_map/all_to_all | solution.py:110
  188.4 25.6 %all-to-all-start.3 = ((bf16[8,96,512]{2,1,0:T(8,128)(2,1)}), bf16[8,96,512]{2,1,0:T(8,128)(2,1)S(1)}, u32[]{:S(2)}, u32[]{:S(2)}) async-start(bf16[8,96,512]{2,1,0:T(8,128)(2,1)} %bitcast.95), calls=%async_computation.4 | async-start | bytes 1572864 | tf_op jit(solution)/shard_map/all_to_all | solution.py:103
  193.0 5.1 %copy-start.2 = (bf16[8,96,2048]{2,1,0:T(8,128)(2,1)S(1)}, bf16[8,96,2048]{2,1,0:T(8,128)(2,1)}, u32[]{:S(2)}) copy-start(bf16[8,96,2048]{2,1,0:T(8,128)(2,1)} %all-gather.5.cloned.1.call-done) | copy-start | bytes 9437188
  198.2 3.1 %copy-start.9 = (bf16[8,96,2048]{2,1,0:T(8,128)(2,1)S(1)}, bf16[8,96,2048]{2,1,0:T(8,128)(2,1)}, u32[]{:S(2)}) copy-start(bf16[8,96,2048]{2,1,0:T(8,128)(2,1)} %all-gather.3.cloned.1.call-done) | copy-start | bytes 9437188
  198.2 3.1 %copy-start.10 = (f32[8,1,96,384]{3,2,0,1:T(8,128)S(1)}, f32[8,1,96,384]{3,2,0,1:T(8,128)}, u32[]{:S(2)}) copy-start(f32[8,1,96,384]{3,2,0,1:T(8,128)} %fusion.13) | copy-start | bytes 3538948
  198.2 3.1 %copy-start.11 = (f32[8,1,96,384]{3,2,0,1:T(8,128)S(1)}, f32[8,1,96,384]{3,2,0,1:T(8,128)}, u32[]{:S(2)}) copy-start(f32[8,1,96,384]{3,2,0,1:T(8,128)} %fusion.16) | copy-start | bytes 3538948
Sparse Core Ops, SparseCore 0:
  44.8 42.6 all-gather.4
  89.3 43.6 all-gather.2
  143.9 44.4 reduce-scatter.1
where the time goes:
time: 225 us; the launch traced here: 224 us
  blocking collectives  86 us (38%)
  waiting for transfers between devices  58.7 us (26%)
  matrix products  30.3 us (13%)
  local copies, waits for them, and re-layouts  22.3 us (10%)
  between operations  14 us (6%)
  starting transfers between devices  9.36 us (4%)
  other arithmetic  3.79 us (2%)
    all_gather x1, waiting for transfers between devices, local(): lax.all_gather(part_grad, 'tp', axis=2, tiled=True)  29.6 us
    all_to_all x1, blocking collectives, local(): lax.all_to_all(pick_rows(token_slice, slot_token, n_experts, capacity), '...  27.3 us
    all_to_all x1, blocking collectives, local(): lax.all_to_all(pick_rows(mix_grad, slot_token, n_experts, capacity), 'ep'...  24 us
    reduce_scatter x1, waiting for transfers between devices, local(): lax.psum_scatter(partial_value.astype(jnp.bfloat16), 'tp', scatter_dimens...  17.9 us
    psum x1, blocking collectives, local(): gate_total = lax.psum(gate_part, 'tp').astype(jnp.bfloat16)  16.7 us
    psum x1, blocking collectives, local(): lax.psum((jnp.sum(mixed * mixed, axis=1), jnp.sum(scaled_grad * mixed, ax...  10 us
    all_to_all x1, blocking collectives, local(): lax.all_to_all(send_weight, 'ep', split_axis=0, concat_axis=0, tiled=True)  7.94 us
    all_to_all x1, waiting for transfers between devices, local(): lax.all_to_all(slot_grad.reshape(ep_count * exp_local, capacity, col_widt...  5.65 us
  transfers between devices with their start and end apart: 5, of which 4 were waited for; matrix products, arithmetic and copies ran while one was open for 14% of the time, Pallas kernels for 0%

commit v1 on v0

--- a/solution.py
+++ b/solution.py
@@ -1,9 +1,277 @@
+import functools
+
 import jax
 import jax.numpy as jnp
 from jax import lax
+from jax.experimental import pallas as pl
+from jax.experimental.pallas import tpu as pltpu
 from jax.sharding import PartitionSpec as P
 
 EPSILON = 0.25
+GROUPS = 4
+CORES = 2
+LANES = 128
+MESH = pl.DeviceIdType.MESH
+VMEM_SPEC = pl.BlockSpec(memory_space=pltpu.VMEM)
+F32 = jnp.float32
+BF16 = jnp.bfloat16
+
+
+def places(zs):
+    ep = lax.axis_index("ep")
+    tp = lax.axis_index("tp")
+    z = ep // CORES
+    core = ep % CORES
+    near_x = tp + 1 - 2 * (tp % 2)
+    near_y = (tp + 2) % 4
+    diag = (near_x + 2) % 4
+    return ep, tp, z, core, near_x, near_y, diag
+
+
+def greet(zs):
+    ep, tp, z, core, near_x, near_y, diag = places(zs)
+    barrier = pltpu.get_barrier_semaphore()
+    peers = [(z * CORES + 1 - core, tp), (ep, near_x), (ep, near_y), (ep, diag)]
+    peers += [(((z + k) % zs) * CORES + core, tp) for k in range(1, zs)]
+    for peer in peers:
+        pl.semaphore_signal(barrier, inc=1, device_id=peer, device_id_type=MESH)
+    pl.semaphore_wait(barrier, len(peers))
+
+
+class Sender:
+    def __init__(self, send_sem):
+        self.send_sem, self.started = send_sem, []
+
+    def __call__(self, src, dst, recv_sem, device):
+        copy = pltpu.make_async_remote_copy(
+            src_ref=src,
+            dst_ref=dst,
+            send_sem=self.send_sem.at[len(self.started)],
+            recv_sem=recv_sem,
+            device_id=device,
+            device_id_type=MESH,
+        )
+        copy.start()
+        self.started.append(copy)
+        return copy
+
+    def finish(self):
+        for copy in self.started:
+            copy.wait_send()
+
+
+def dispatch_kernel(
+    zs, cap, width,
+    tok_ref, moe_ref, grad_ref, gain_ref, perm_ref, wmat_ref,
+    x_ref, g_ref, w_ref,
+    pack_x, pack_g, pack_w, stats,
+    send_sem, stat_sem, z_sem, w_sem, wp_sem, tp_sem, pair_sem,
+):
+    ep, tp, z, core, near_x, near_y, diag = places(zs)
+    n_tok, full = tok_ref.shape
+    partner = (z * CORES + 1 - core, tp)
+    send = Sender(send_sem)
+
+    def cols(at):
+        return pl.ds(pl.multiple_of(at * width, width), width)
+
+    def rows(source, who=None):
+        start = (source * CORES + (core if who is None else who)) * cap
+        return pl.ds(pl.multiple_of(start, 16), cap)
+
+    def chip_rows(q):
+        return pl.ds(pl.multiple_of(q * cap, 16), cap)
+
+    mixed = moe_ref[...].astype(F32)
+    scaled = grad_ref[...].astype(F32) * gain_ref[...]
+    squares = jnp.sum(mixed * mixed, axis=1, keepdims=True)
+    crossed = jnp.sum(scaled * mixed, axis=1, keepdims=True)
+    lane = lax.broadcasted_iota(jnp.int32, (n_tok, LANES), 1)
+    both = jnp.where(lane == 0, squares, jnp.where(lane == 1, crossed, 0.0))
+    tall = stats.shape[2]
+    both = jnp.concatenate([both, jnp.zeros((tall - n_tok, LANES), F32)], axis=0)
+    stats[0] = both.T[:8]
+    greet(zs)
+    got_stats = [
+        send(stats.at[0], stats.at[1 + i], stat_sem.at[i], (ep, to))
+        for i, to in enumerate((near_x, near_y, diag))
+    ]
+
+    tok = tok_ref[:, cols(tp)]
+    perm = perm_ref[...]
+    pack_x[...] = jnp.dot(perm, tok, preferred_element_type=F32).astype(BF16)
+    pack_w[...] = jnp.dot(perm, wmat_ref[...], preferred_element_type=F32).astype(BF16)
+    x_ref[rows(z), cols(tp)] = pack_x[chip_rows(z), :]
+    w_ref[rows(z), :] = pack_w[chip_rows(z), :]
+    outs, packs = (x_ref, g_ref), (pack_x, pack_g)
+    z_copies, w_copies = {}, {}
+
+    def z_out(t):
+        for k in range(1, zs):
+            q = (z + k) % zs
+            z_copies[t, k] = send(
+                packs[t].at[chip_rows(q)],
+                outs[t].at[rows(z), cols(tp)],
+                z_sem.at[t, k],
+                (q * CORES + core, tp),
+            )
+
+    z_out(0)
+    for k in range(1, zs):
+        q = (z + k) % zs
+        w_copies[k] = send(
+            pack_w.at[chip_rows(q)], w_ref.at[rows(z)], w_sem.at[k], (q * CORES + core, tp)
+        )
+
+    tp_copies, pair_copies = {}, []
+
+    def to_pair(t, k, origin, at):
+        block = outs[t].at[rows((z - k + zs) % zs), cols(at)]
+        pair_copies.append(send(block, block, pair_sem.at[t, k, origin], partner))
+
+    def arrive(t, k):
+        if k:
+            z_copies[t, k].wait_recv()
+        block = outs[t].at[rows((z - k + zs) % zs), cols(tp)]
+        tp_copies[t, k, 0] = send(block, block, tp_sem.at[t, k, 0], (ep, near_x))
+        tp_copies[t, k, 1] = send(block, block, tp_sem.at[t, k, 1], (ep, near_y))
+        to_pair(t, k, 0, tp)
+
+    def relay(t, k):
+        tp_copies[t, k, 0].wait_recv()
+        tp_copies[t, k, 1].wait_recv()
+        at, to = ((near_x, near_y), (near_y, near_x))[t]
+        block = outs[t].at[rows((z - k + zs) % zs), cols(at)]
+        tp_copies[t, k, 2] = send(block, block, tp_sem.at[t, k, 2], (ep, to))
+        to_pair(t, k, 1, near_x)
+        to_pair(t, k, 2, near_y)
+
+    arrive(0, 0)
+    for copy in got_stats:
+        copy.wait_recv()
+    total = stats[0] + stats[1] + stats[2] + stats[3]
+    total = jnp.concatenate([total, jnp.zeros((LANES - 8, tall), F32)], axis=0).T[:n_tok]
+    inverse = lax.rsqrt(total[:, 0:1] / full + EPSILON)
+    coupling = inverse * inverse * inverse * (total[:, 1:2] / full)
+    mix = (inverse * scaled - mixed * coupling).astype(BF16)
+    pack_g[...] = jnp.dot(perm, mix, preferred_element_type=F32).astype(BF16)
+    g_ref[rows(z), cols(tp)] = pack_g[chip_rows(z), :]
+    z_out(1)
+    arrive(1, 0)
+
+    pair_w = [send(w_ref.at[rows(z)], w_ref.at[rows(z)], wp_sem.at[0], partner)]
+    for k in range(1, zs):
+        for t in range(2):
+            arrive(t, k)
+            relay(t, k - 1)
+        w_copies[k].wait_recv()
+        block = w_ref.at[rows((z - k + zs) % zs)]
+        pair_w.append(send(block, block, wp_sem.at[k], partner))
+    for t in range(2):
+        relay(t, zs - 1)
+    for k in range(zs):
+        for t in range(2):
+            tp_copies[t, k, 2].wait_recv()
+            to_pair(t, k, 3, diag)
+    for copy in pair_w + pair_copies:
+        copy.wait_recv()
+    send.finish()
+
+
+def return_kernel(
+    zs, cap, width,
+    part_ref, gate_ref,
+    back_ref, total_ref,
+    comb, pin, first_in, second_out, second_in, final, gates,
+    send_sem, pin_sem, one_sem, two_sem, z_sem, gate_sem, gz_sem,
+):
+    ep, tp, z, core, near_x, near_y, diag = places(zs)
+    partner = (z * CORES + 1 - core, tp)
+    send = Sender(send_sem)
+    half = width // 2
+    order = list(range(1, zs)) + [0]
+
+    def rows(source, who):
+        return pl.ds(pl.multiple_of((source * CORES + who) * cap, 16), cap)
+
+    def chip_rows(q):
+        return pl.ds(pl.multiple_of(q * cap, 16), cap)
+
+    def cols(at, which):
+        return pl.ds(pl.multiple_of(at * width + which * half, half), half)
+
+    gates[0, core] = gate_ref[...]
+    greet(zs)
+    pin_copies, one, two, back = {}, {}, {}, {}
+    pair_gate = send(gate_ref, gates.at[0, core], gate_sem.at[3], partner)
+    for k in order:
+        q = (z + k) % zs
+        pin_copies[k] = send(
+            part_ref.at[rows(q, 1 - core)], pin.at[k], pin_sem.at[k], partner
+        )
+    pair_gate.wait_recv()
+    gate_copies = [
+        send(gates.at[0], gates.at[1 + i], gate_sem.at[i], (ep, to))
+        for i, to in enumerate((near_x, near_y, diag))
+    ]
+
+    def stage_one(k):
+        q = (z + k) % zs
+        pin_copies[k].wait_recv()
+        comb[k] = (part_ref[rows(q, core), :].astype(F32) + pin[k].astype(F32)).astype(BF16)
+        for which, near in enumerate((near_x, near_y)):
+            for i, at in enumerate((near, diag)):
+                one[k, which, i] = send(
+                    comb.at[k, :, cols(at, which)],
+                    first_in.at[k, which, i],
+                    one_sem.at[k, which, i],
+                    (ep, near),
+                )
+
+    def stage_two(k):
+        for which, far in enumerate((near_y, near_x)):
+            one[k, which, 1].wait_recv()
+            second_out[k, which] = (
+                comb[k, :, cols(far, which)].astype(F32) + first_in[k, which, 1].astype(F32)
+            ).astype(BF16)
+            two[k, which] = send(
+                second_out.at[k, which], second_in.at[k, which], two_sem.at[k, which], (ep, far)
+            )
+
+    def stage_three(k):
+        q = (z + k) % zs
+        for which in range(2):
+            one[k, which, 0].wait_recv()
+            two[k, which].wait_recv()
+            final[k, :, which * half : (which + 1) * half] = (
+                comb[k, :, cols(tp, which)].astype(F32)
+                + first_in[k, which, 0].astype(F32)
+                + second_in[k, which].astype(F32)
+            ).astype(BF16)
+        if k:
+            back[k] = send(
+                final.at[k], back_ref.at[chip_rows(z)], z_sem.at[k], (q * CORES + core, tp)
+            )
+        else:
+            back_ref[chip_rows(z), :] = final[0]
+
+    for k in order:
+        stage_one(k)
+    for copy in gate_copies:
+        copy.wait_recv()
+    total_ref[z] = gates[0] + gates[1] + gates[2] + gates[3]
+    gate_back = [
+        send(total_ref.at[z], total_ref.at[z], gz_sem.at[k], (((z + k) % zs) * CORES + core, tp))
+        for k in range(1, zs)
+    ]
+    for at, k in enumerate(order):
+        stage_two(k)
+        if at:
+            stage_three(order[at - 1])
+    stage_three(order[-1])
+    for copy in list(back.values()) + gate_back:
+        copy.wait_recv()
+    send.finish()
 
 
 def pick_rows(matrix, slot_token, n_experts, capacity):
@@ -11,7 +279,7 @@
     return padded[slot_token].reshape(n_experts, capacity, matrix.shape[1])
 
 
-def local(tokens, moe_out, out_grad, norm_gain, gate_weights, expert_ids, gate_w, up_w, down_w):
+def general(tokens, moe_out, out_grad, norm_gain, gate_weights, expert_ids, gate_w, up_w, down_w):
     tok_count = tokens.shape[0]
     full_width = tokens.shape[1]
     col_width = moe_out.shape[1]
@@ -123,6 +391,144 @@
     return (token_grad, gate_grad, gate_grad_w, up_grad_w, down_grad)
 
 
+def local(tokens, moe_out, out_grad, norm_gain, gate_weights, expert_ids, gate_w, up_w, down_w):
+    tok_count, full_width = tokens.shape
+    width = moe_out.shape[1]
+    ep_count = lax.axis_size("ep")
+    exp_local = gate_w.shape[0]
+    if exp_local != 1 or lax.axis_size("tp") != 4 or ep_count % CORES:
+        return general(
+            tokens, moe_out, out_grad, norm_gain, gate_weights, expert_ids, gate_w, up_w, down_w
+        )
+    n_experts = ep_count * exp_local
+    top_count = expert_ids.shape[1]
+    expert_cap = 2 * tok_count * top_count // n_experts
+    zs = ep_count // CORES
+    cap = expert_cap if n_experts // GROUPS <= CORES else CORES * expert_cap
+    slots = ep_count * cap
+
+    chip_of = expert_ids // CORES
+    chips = jnp.arange(zs, dtype=jnp.int32)
+    named = chip_of[:, :, None] == chips
+    member = jnp.any(named, axis=1)
+    earlier = (
+        jnp.arange(tok_count, dtype=jnp.int32)[:, None]
+        > jnp.arange(tok_count, dtype=jnp.int32)[None, :]
+    ).astype(BF16)
+    rank = jnp.dot(earlier, member.astype(BF16), preferred_element_type=F32).astype(jnp.int32)
+    slot_of = jnp.where(member, rank, -1)
+    places_at = jnp.arange(cap, dtype=jnp.int32)
+    perm = (
+        (slot_of.T[:, None, :] == places_at[None, :, None]).astype(BF16).reshape(zs * cap, tok_count)
+    )
+    chosen = expert_ids[:, :, None] == jnp.arange(LANES, dtype=jnp.int32)
+    wmat = jnp.sum(jnp.where(chosen, gate_weights[:, :, None].astype(F32), 0.0), axis=1).astype(BF16)
+
+    n_send = 3 + 3 * (zs - 1) + zs + 2 * zs * 7
+    inputs, cotangent, weights = pl.pallas_call(
+        functools.partial(dispatch_kernel, zs, cap, width),
+        out_shape=(
+            jax.ShapeDtypeStruct((slots, full_width), BF16),
+            jax.ShapeDtypeStruct((slots, full_width), BF16),
+            jax.ShapeDtypeStruct((slots, LANES), BF16),
+        ),
+        in_specs=[VMEM_SPEC] * 6,
+        out_specs=(VMEM_SPEC,) * 3,
+        scratch_shapes=[
+            pltpu.VMEM((zs * cap, width), BF16),
+            pltpu.VMEM((zs * cap, width), BF16),
+            pltpu.VMEM((zs * cap, LANES), BF16),
+            pltpu.VMEM((4, 8, -(-tok_count // LANES) * LANES), F32),
+            pltpu.SemaphoreType.DMA((n_send,)),
+            pltpu.SemaphoreType.DMA((3,)),
+            pltpu.SemaphoreType.DMA((2, zs)),
+            pltpu.SemaphoreType.DMA((zs,)),
+            pltpu.SemaphoreType.DMA((zs,)),
+            pltpu.SemaphoreType.DMA((2, zs, 3)),
+            pltpu.SemaphoreType.DMA((2, zs, 4)),
+        ],
+        compiler_params=pltpu.CompilerParams(
+            collective_id=0, has_side_effects=True, vmem_limit_bytes=48 * 1024 * 1024
+        ),
+    )(tokens, moe_out, out_grad, norm_gain.reshape(1, width), perm, wmat)
+
+    core = lax.axis_index("ep")
+    lane = jnp.arange(LANES, dtype=jnp.int32)
+    scales = jnp.sum(
+        jnp.where(lane == core, weights.astype(F32), 0.0), axis=1, keepdims=True
+    )
+    w_gate, w_up, w_down = gate_w[0], up_w[0], down_w[0]
+
+    def contract(a, b, dims):
+        return lax.dot_general(a, b, (dims, ((), ())), preferred_element_type=F32)
+
+    gate_pre = contract(inputs, w_gate, ((1,), (1,)))
+    up_pre = contract(inputs, w_up, ((1,), (1,)))
+    hidden_grad = contract(cotangent, w_down, ((1,), (1,)))
+    sigmoid = jax.nn.sigmoid(gate_pre)
+    activated = gate_pre * sigmoid
+    gate_part = jnp.sum(activated * up_pre * hidden_grad, axis=1).reshape(ep_count, cap)
+    gate_part = jnp.pad(gate_part, ((0, 0), (0, LANES - cap)))
+    scaled_hidden = (scales * activated * up_pre).astype(BF16)
+    gate_delta = (
+        scales * hidden_grad * up_pre * sigmoid * (1.0 + gate_pre * (1.0 - sigmoid))
+    ).astype(BF16)
+    up_delta = (scales * hidden_grad * activated).astype(BF16)
+    partial_value = (
+        contract(gate_delta, w_gate, ((1,), (0,))) + contract(up_delta, w_up, ((1,), (0,)))
+    ).astype(BF16)
+    down_grad = contract(scaled_hidden, cotangent, ((0,), (0,)))[None]
+    gate_grad_w = contract(gate_delta, inputs, ((0,), (0,)))[None]
+    up_grad_w = contract(up_delta, inputs, ((0,), (0,)))[None]
+
+    half = width // 2
+    n_send = 4 + zs + 4 * zs + 2 * zs + 2 * (zs - 1)
+    back, totals = pl.pallas_call(
+        functools.partial(return_kernel, zs, cap, width),
+        out_shape=(
+            jax.ShapeDtypeStruct((zs * cap, width), BF16),
+            jax.ShapeDtypeStruct((zs, CORES, ep_count, LANES), F32),
+        ),
+        in_specs=[VMEM_SPEC] * 2,
+        out_specs=(VMEM_SPEC,) * 2,
+        scratch_shapes=[
+            pltpu.VMEM((zs, cap, full_width), BF16),
+            pltpu.VMEM((zs, cap, full_width), BF16),
+            pltpu.VMEM((zs, 2, 2, cap, half), BF16),
+            pltpu.VMEM((zs, 2, cap, half), BF16),
+            pltpu.VMEM((zs, 2, cap, half), BF16),
+            pltpu.VMEM((zs, cap, width), BF16),
+            pltpu.VMEM((4, CORES, ep_count, LANES), F32),
+            pltpu.SemaphoreType.DMA((n_send,)),
+            pltpu.SemaphoreType.DMA((zs,)),
+            pltpu.SemaphoreType.DMA((zs, 2, 2)),
+            pltpu.SemaphoreType.DMA((zs, 2)),
+            pltpu.SemaphoreType.DMA((zs,)),
+            pltpu.SemaphoreType.DMA((4,)),
+            pltpu.SemaphoreType.DMA((zs,)),
+        ],
+        compiler_params=pltpu.CompilerParams(
+            collective_id=1, has_side_effects=True, vmem_limit_bytes=48 * 1024 * 1024
+        ),
+    )(partial_value, gate_part)
+
+    token_grad = contract(perm, back, ((0,), (0,))).astype(BF16)
+    me = lax.axis_index("ep")
+    mine = lax.dynamic_index_in_dim(totals, me, 2, keepdims=False)[:, :, :cap]
+    mine = mine.astype(BF16).astype(F32)
+    here = slot_of[:, :, None] == places_at
+    parity = expert_ids % CORES
+    columns = []
+    for k in range(top_count):
+        pick = jnp.where(
+            (parity[:, k] == 0)[:, None, None], mine[:, 0][None], mine[:, 1][None]
+        )
+        keep = here & named[:, k][:, :, None]
+        columns.append(jnp.sum(jnp.where(keep, pick, 0.0), axis=(1, 2)))
+    gate_grad = jnp.stack(columns, axis=1).astype(BF16)
+    return (token_grad, gate_grad, gate_grad_w, up_grad_w, down_grad)
+
+
 def solution(mesh):
     in_specs = (
         P("ep", None),

time: 225 us -> 114 us (0.51)
  blocking collectives: 86 us -> 0 us
  Pallas kernels: 0 us -> 73.2 us
  waiting for transfers between devices: 58.7 us -> 0 us
  local copies, waits for them, and re-layouts: 22.3 us -> 5.79 us
  between operations: 14 us -> 0.79 us
  starting transfers between devices: 9.36 us -> 0 us
    pallas_call x0 -> x2, Pallas kernels: none -> 73.2 us  [the longest x1 43.5 us: local(): pl.pallas_call(functools.partial(dispatch_kernel, zs, cap, width), out_sh...]
    all_to_all x3 -> x0, blocking collectives: 59.3 us -> none  [the longest x1 27.3 us: local(): lax.all_to_all(pick_rows(token_slice, slot_token, n_experts, capacity), '...]
    all_gather x2 -> x0, waiting for transfers between devices: 29.6 us -> none  [the longest x1 29.6 us: local(): lax.all_gather(part_grad, 'tp', axis=2, tiled=True)]
    psum x2 -> x0, blocking collectives: 26.7 us -> none  [the longest x1 16.7 us: local(): gate_total = lax.psum(gate_part, 'tp').astype(jnp.bfloat16)]
    reduce_scatter x1 -> x0, waiting for transfers between devices: 17.9 us -> none  [local(): lax.psum_scatter(partial_value.astype(jnp.bfloat16), 'tp', scatter_dimens...]
    gather x5 -> x0, local copies, waits for them, and re-layouts: 15.2 us -> none  [the longest x2 5.36 us: pick_rows(): return padded[slot_token].reshape(n_experts, capacity, matrix.shape[1])]
    all_to_all x2 -> x0, waiting for transfers between devices: 11.2 us -> none  [the longest x1 5.65 us: local(): lax.all_to_all(slot_grad.reshape(ep_count * exp_local, capacity, col_widt...]
    all_to_all x2 -> x0, starting transfers between devices: 9.23 us -> none  [the longest x1 4.63 us: local(): lax.all_to_all(slot_grad.reshape(ep_count * exp_local, capacity, col_widt...]
  transfers between devices with their start and end apart: 5 -> 0, of which waited for: 4 -> 0; matrix products, arithmetic and copies ran while one was open for 14% -> 0% of each run, Pallas kernels for 0% -> 0%
where the time goes in v1:
time: 114 us
  Pallas kernels  73.2 us (64%)
  matrix products  30.3 us (27%)
  local copies, waits for them, and re-layouts  5.79 us (5%)
  other arithmetic  3.82 us (3%)
    pallas_call x1, Pallas kernels, local(): pl.pallas_call(functools.partial(dispatch_kernel, zs, cap, width), out_sh...  43.5 us
    dot_general x9, matrix products, contract(): return lax.dot_general(a, b, (dims, ((), ())), preferred_element_type=F32)  30.1 us
    pallas_call x1, Pallas kernels, local(): pl.pallas_call(functools.partial(return_kernel, zs, cap, width), out_shap...  29.7 us
    unnamed x25, local copies, waits for them, and re-layouts  5.59 us

profile of v1, /device:TPU:0, one launch (start us, length us, event | category | flops | bytes accessed | tf_op | source)
XLA Modules:
  0.0 113.9 jit_solution(15316367877558826073)
XLA Ops:
  0.7 0.8 and_select_fusion
  1.6 0.1 fusion.10
  1.7 0.2 fusion.14
  1.9 0.7 convert_element_type.45
  2.6 0.8 select_reduce_fusion.3.wmat_ref
  3.4 1.1 copy-done.2
  4.6 0.9 copy-done.3
  5.5 0.9 copy-done.4
  6.4 0.7 copy-done.5
  7.1 43.5 %shard_map.128 = (bf16[768,2048]{1,0:T(8,128)(2,1)S(1)}, bf16[768,2048]{1,0:T(8,128)(2,1)}, bf16[768,128]{1,0:T(8,128)(2,1)S(1)}) custom-call(bf16[192,2048]{1,0:T(8,128)(2,1)S(1)} %copy-done.2, bf16[192,512]{1,0:T(8,128)(2,1)S(1)} %copy-done.3, bf16[192,512]{1,0:T(8,128)(2,1)S(1)} %copy-done.4, f32[1,512]{1,0:T(1,128)S(1)} %bitcast.49, ...), custom_call_target="tpu_custom_call" | custom-call | tf_op jit(solution)/shard_map/pallas_call | solution.py:428
  50.6 5.0 %fusion.5 = f32[768,384]{0,1:T(8,128)} fusion(bf16[768,2048]{1,0:T(8,128)(2,1)S(1)} %get-tuple-element.12, bf16[1,384,2048]{2,1,0:T(8,128)(2,1)} %param.16), kind=kOutput, calls=%fused_computation.9 | convolution fusion | flops 1207959552 | bytes 5898240 | tf_op jit(solution)/shard_map/dot_general | solution.py:463
  55.6 2.4 %fusion.2 = f32[768,384]{0,1:T(8,128)} fusion(bf16[768,2048]{1,0:T(8,128)(2,1)S(1)} %get-tuple-element.12, bf16[1,384,2048]{2,1,0:T(8,128)(2,1)S(1)} %copy-done), kind=kOutput, calls=%fused_computation.6 | convolution fusion | flops 1207959552 | bytes 5898240 | tf_op jit(solution)/shard_map/dot_general | solution.py:463
  58.1 0.1 select_reduce_fusion.2
  58.2 4.9 %multiply_reduce_fusion = (f32[768]{0:T(1024)S(1)}, bf16[768,384]{0,1:T(8,128)(2,1)S(1)}, bf16[768,384]{0,1:T(8,128)(2,1)S(1)}) fusion(f32[768,384]{0,1:T(8,128)} %fusion.5, f32[768,384]{0,1:T(8,128)} %fusion.2, f32[768]{0:T(1024)S(1)} %select_reduce_fusion.2, bf16[768,2048]{1,0:T(8,128)(2,1)} %get-tuple-element.11, bf16[1,384,2048]{2,1,0:T(8,128)(2,1)} %param.17), kind=kOutput, calls=%fused_computation.14 | convolution fusion | flops 1212972288 | bytes 8263680 | tf_op jit(solution)/shard_map/dot_general | solution.py:463
  63.1 1.8 %fusion = f32[768,2048]{1,0:T(8,128)S(1)} fusion(bf16[768,384]{0,1:T(8,128)(2,1)S(1)} %get-tuple-element.22, bf16[1,384,2048]{2,1,0:T(8,128)(2,1)S(1)} %copy-done), kind=kOutput, calls=%fused_computation.4 | convolution fusion | flops 1207959552 | bytes 8454144 | tf_op jit(solution)/shard_map/dot_general | solution.py:463
  65.0 3.5 %add_convert_fusion.part_ref = bf16[768,2048]{1,0:T(8,128)(2,1)} fusion(f32[768,2048]{1,0:T(8,128)S(1)} %fusion, bf16[768,384]{0,1:T(8,128)(2,1)S(1)} %get-tuple-element.23, bf16[1,384,2048]{2,1,0:T(8,128)(2,1)S(1)} %copy-done.8), kind=kOutput, calls=%fused_computation | convolution fusion | flops 1211105280 | bytes 11599872 | tf_op jit(solution)/shard_map/dot_general | solution.py:463
  68.6 1.9 %copy-done.1 = bf16[768,2048]{1,0:T(8,128)(2,1)S(1)} copy-done((bf16[768,2048]{1,0:T(8,128)(2,1)S(1)}, bf16[768,2048]{1,0:T(8,128)(2,1)}, u32[]{:S(2)}) %copy-start.1) | copy-done | bytes 3145752
  70.5 29.7 %shard_map.129 = (bf16[384,512]{1,0:T(8,128)(2,1)S(1)}, f32[4,2,8,128]{3,2,1,0:T(8,128)S(1)}) custom-call(bf16[768,2048]{1,0:T(8,128)(2,1)S(1)} %copy-done.1, f32[8,128]{1,0:T(8,128)S(1)} %pad.4.gate_ref), custom_call_target="tpu_custom_call" | custom-call | tf_op jit(solution)/shard_map/pallas_call | solution.py:486
  100.2 1.0 convolution_convert_fusion
  101.3 0.6 select_reduce_fusion.1
  101.9 0.6 pad_maximum_fusion
  102.4 5.3 %convolution_bitcast_fusion.2 = f32[1,384,2048]{2,1,0:T(8,128)} fusion(bf16[768,384]{0,1:T(8,128)(2,1)S(1)} %get-tuple-element.22, bf16[768,2048]{1,0:T(8,128)(2,1)} %copy-done.6), kind=kOutput, calls=%fused_computation.3 | convolution fusion | flops 1207959552 | bytes 6881280 | tf_op jit(solution)/shard_map/dot_general | solution.py:463
  107.7 3.1 %convolution_bitcast_fusion.1 = f32[1,384,2048]{2,1,0:T(8,128)} fusion(bf16[768,384]{0,1:T(8,128)(2,1)S(1)} %get-tuple-element.23, bf16[768,2048]{1,0:T(8,128)(2,1)S(1)} %copy-done.7), kind=kOutput, calls=%fused_computation.2 | convolution fusion | flops 1207959552 | bytes 6881280 | tf_op jit(solution)/shard_map/dot_general | solution.py:463
  110.8 3.1 %convolution_bitcast_fusion = f32[1,384,2048]{2,1,0:T(8,128)} fusion(bf16[768,2048]{1,0:T(8,128)(2,1)S(1)} %copy-done.9, f32[768,384]{0,1:T(8,128)S(1)} %copy-done.10, f32[768]{0:T(1024)S(1)} %select_reduce_fusion.2, f32[768,384]{0,1:T(8,128)S(1)} %copy-done.11), kind=kOutput, calls=%fused_computation.1 | convolution fusion | flops 1210023936 | bytes 8653824 | tf_op jit(solution)/shard_map/dot_general | solution.py:463
  (33 shorter events, 0.3 us)
Async XLA Ops:
  0.6 55.0 %copy-start = (bf16[1,384,2048]{2,1,0:T(8,128)(2,1)S(1)}, bf16[1,384,2048]{2,1,0:T(8,128)(2,1)}, u32[]{:S(2)}) copy-start(bf16[1,384,2048]{2,1,0:T(8,128)(2,1)} %param.15) | copy-start | bytes 4718596
  3.4 1.1 copy-start.2
  4.6 0.9 copy-start.3
  5.5 0.9 copy-start.4
  6.4 0.7 copy-start.5
  50.6 5.0 %copy-start.6 = (bf16[768,2048]{1,0:T(8,128)(2,1)}, bf16[768,2048]{1,0:T(8,128)(2,1)S(1)}, u32[]{:S(2)}) copy-start(bf16[768,2048]{1,0:T(8,128)(2,1)S(1)} %get-tuple-element.12) | copy-start | bytes 9437188
  63.1 1.8 %copy-start.8 = (bf16[1,384,2048]{2,1,0:T(8,128)(2,1)S(1)}, bf16[1,384,2048]{2,1,0:T(8,128)(2,1)}, u32[]{:S(2)}) copy-start(bf16[1,384,2048]{2,1,0:T(8,128)(2,1)} %param.16) | copy-start | bytes 4718596
  68.6 1.9 %copy-start.1 = (bf16[768,2048]{1,0:T(8,128)(2,1)S(1)}, bf16[768,2048]{1,0:T(8,128)(2,1)}, u32[]{:S(2)}) copy-start(bf16[768,2048]{1,0:T(8,128)(2,1)} %add_convert_fusion.part_ref) | copy-start | bytes 9437188
  102.4 5.3 %copy-start.7 = (bf16[768,2048]{1,0:T(8,128)(2,1)S(1)}, bf16[768,2048]{1,0:T(8,128)(2,1)}, u32[]{:S(2)}) copy-start(bf16[768,2048]{1,0:T(8,128)(2,1)} %copy-done.6) | copy-start | bytes 9437188
  107.7 3.1 %copy-start.9 = (bf16[768,2048]{1,0:T(8,128)(2,1)S(1)}, bf16[768,2048]{1,0:T(8,128)(2,1)}, u32[]{:S(2)}) copy-start(bf16[768,2048]{1,0:T(8,128)(2,1)} %get-tuple-element.11) | copy-start | bytes 9437188
  107.7 3.1 %copy-start.10 = (f32[768,384]{0,1:T(8,128)S(1)}, f32[768,384]{0,1:T(8,128)}, u32[]{:S(2)}) copy-start(f32[768,384]{0,1:T(8,128)} %fusion.5) | copy-start | bytes 3538948
  107.7 3.1 %copy-start.11 = (f32[768,384]{0,1:T(8,128)S(1)}, f32[768,384]{0,1:T(8,128)}, u32[]{:S(2)}) copy-start(f32[768,384]{0,1:T(8,128)} %fusion.2) | copy-start | bytes 3538948

commit v2 on v1

--- a/solution.py
+++ b/solution.py
@@ -60,28 +60,50 @@
             copy.wait_send()
 
 
-def dispatch_kernel(
+def route_kernel(
     zs, cap, width,
-    tok_ref, moe_ref, grad_ref, gain_ref, perm_ref, wmat_ref,
-    x_ref, g_ref, w_ref,
-    pack_x, pack_g, pack_w, stats,
-    send_sem, stat_sem, z_sem, w_sem, wp_sem, tp_sem, pair_sem,
+    tok_hbm, moe_hbm, grad_hbm, gain_ref, perm_ref, wmat_ref, wg_hbm, wu_hbm, wd_hbm,
+    back_ref, total_ref, dwg_ref, dwu_ref, dwd_ref,
+    tok_ref, moe_ref, grad_ref, wg_ref, wu_ref, wd_ref, x_ref, g_ref, w_ref,
+    pack_x, pack_g, pack_w, stats, hid_ref, gd_ref, ud_ref,
+    part_ref, comb, pin, first_in, second_out, second_in, final, gates,
+    load_sem, send_sem, stat_sem, z_sem, w_sem, wp_sem, tp_sem, pair_sem,
+    pin_sem, one_sem, two_sem, back_sem, gate_sem, gz_sem,
 ):
     ep, tp, z, core, near_x, near_y, diag = places(zs)
-    n_tok, full = tok_ref.shape
+    n_tok = tok_ref.shape[0]
+    full = x_ref.shape[1]
     partner = (z * CORES + 1 - core, tp)
     send = Sender(send_sem)
+    half = width // 2
 
     def cols(at):
         return pl.ds(pl.multiple_of(at * width, width), width)
 
-    def rows(source, who=None):
-        start = (source * CORES + (core if who is None else who)) * cap
+    def half_cols(at, which):
+        return pl.ds(pl.multiple_of(at * width + which * half, half), half)
+
+    def source(k):
+        return (z - k + zs) % zs
+
+    def rows(q, who=None):
+        start = (q * CORES + (core if who is None else who)) * cap
         return pl.ds(pl.multiple_of(start, 16), cap)
 
     def chip_rows(q):
         return pl.ds(pl.multiple_of(q * cap, 16), cap)
 
+    loads = [
+        pltpu.make_async_copy(src, dst, load_sem.at[i])
+        for i, (src, dst) in enumerate((
+            (moe_hbm, moe_ref), (grad_hbm, grad_ref), (tok_hbm.at[:, cols(tp)], tok_ref),
+            (wg_hbm, wg_ref), (wu_hbm, wu_ref), (wd_hbm, wd_ref),
+        ))
+    ]
+    for load in loads:
+        load.start()
+    loads[0].wait()
+    loads[1].wait()
     mixed = moe_ref[...].astype(F32)
     scaled = grad_ref[...].astype(F32) * gain_ref[...]
     squares = jnp.sum(mixed * mixed, axis=1, keepdims=True)
@@ -97,9 +119,9 @@
         for i, to in enumerate((near_x, near_y, diag))
     ]
 
-    tok = tok_ref[:, cols(tp)]
+    loads[2].wait()
     perm = perm_ref[...]
-    pack_x[...] = jnp.dot(perm, tok, preferred_element_type=F32).astype(BF16)
+    pack_x[...] = jnp.dot(perm, tok_ref[...], preferred_element_type=F32).astype(BF16)
     pack_w[...] = jnp.dot(perm, wmat_ref[...], preferred_element_type=F32).astype(BF16)
     x_ref[rows(z), cols(tp)] = pack_x[chip_rows(z), :]
     w_ref[rows(z), :] = pack_w[chip_rows(z), :]
@@ -117,22 +139,16 @@
             )
 
     z_out(0)
-    for k in range(1, zs):
-        q = (z + k) % zs
-        w_copies[k] = send(
-            pack_w.at[chip_rows(q)], w_ref.at[rows(z)], w_sem.at[k], (q * CORES + core, tp)
-        )
-
-    tp_copies, pair_copies = {}, []
+    tp_copies, pair_copies = {}, {}
 
     def to_pair(t, k, origin, at):
-        block = outs[t].at[rows((z - k + zs) % zs), cols(at)]
-        pair_copies.append(send(block, block, pair_sem.at[t, k, origin], partner))
+        block = outs[t].at[rows(source(k)), cols(at)]
+        pair_copies[t, k, origin] = send(block, block, pair_sem.at[t, k, origin], partner)
 
     def arrive(t, k):
         if k:
             z_copies[t, k].wait_recv()
-        block = outs[t].at[rows((z - k + zs) % zs), cols(tp)]
+        block = outs[t].at[rows(source(k)), cols(tp)]
         tp_copies[t, k, 0] = send(block, block, tp_sem.at[t, k, 0], (ep, near_x))
         tp_copies[t, k, 1] = send(block, block, tp_sem.at[t, k, 1], (ep, near_y))
         to_pair(t, k, 0, tp)
@@ -141,7 +157,7 @@
         tp_copies[t, k, 0].wait_recv()
         tp_copies[t, k, 1].wait_recv()
         at, to = ((near_x, near_y), (near_y, near_x))[t]
-        block = outs[t].at[rows((z - k + zs) % zs), cols(at)]
+        block = outs[t].at[rows(source(k)), cols(at)]
         tp_copies[t, k, 2] = send(block, block, tp_sem.at[t, k, 2], (ep, to))
         to_pair(t, k, 1, near_x)
         to_pair(t, k, 2, near_y)
@@ -157,106 +173,152 @@
     pack_g[...] = jnp.dot(perm, mix, preferred_element_type=F32).astype(BF16)
     g_ref[rows(z), cols(tp)] = pack_g[chip_rows(z), :]
     z_out(1)
-    arrive(1, 0)
-
-    pair_w = [send(w_ref.at[rows(z)], w_ref.at[rows(z)], wp_sem.at[0], partner)]
     for k in range(1, zs):
-        for t in range(2):
-            arrive(t, k)
-            relay(t, k - 1)
-        w_copies[k].wait_recv()
-        block = w_ref.at[rows((z - k + zs) % zs)]
-        pair_w.append(send(block, block, wp_sem.at[k], partner))
-    for t in range(2):
-        relay(t, zs - 1)
-    for k in range(zs):
+        q = (z + k) % zs
+        w_copies[k] = send(
+            pack_w.at[chip_rows(q)], w_ref.at[rows(z)], w_sem.at[k], (q * CORES + core, tp)
+        )
+
+    def last_part(k):
         for t in range(2):
             tp_copies[t, k, 2].wait_recv()
             to_pair(t, k, 3, diag)
-    for copy in pair_w + pair_copies:
-        copy.wait_recv()
-    send.finish()
-
-
-def return_kernel(
-    zs, cap, width,
-    part_ref, gate_ref,
-    back_ref, total_ref,
-    comb, pin, first_in, second_out, second_in, final, gates,
-    send_sem, pin_sem, one_sem, two_sem, z_sem, gate_sem, gz_sem,
-):
-    ep, tp, z, core, near_x, near_y, diag = places(zs)
-    partner = (z * CORES + 1 - core, tp)
-    send = Sender(send_sem)
-    half = width // 2
-    order = list(range(1, zs)) + [0]
-
-    def rows(source, who):
-        return pl.ds(pl.multiple_of((source * CORES + who) * cap, 16), cap)
-
-    def chip_rows(q):
-        return pl.ds(pl.multiple_of(q * cap, 16), cap)
-
-    def cols(at, which):
-        return pl.ds(pl.multiple_of(at * width + which * half, half), half)
-
-    gates[0, core] = gate_ref[...]
-    greet(zs)
+        if k:
+            w_copies[k].wait_recv()
+        block = w_ref.at[rows(source(k))]
+        pair_copies["w", k] = send(block, block, wp_sem.at[k], partner)
+
+    nt = (((1,), (1,)), ((), ()))
+
+    def compute(k):
+        q = source(k)
+        for t in range(2):
+            for origin in range(4):
+                pair_copies[t, k, origin].wait_recv()
+        pair_copies["w", k].wait_recv()
+        block = pl.ds(pl.multiple_of(q * (CORES * cap), 16), CORES * cap)
+        x = x_ref[block, :]
+        gate_pre = lax.dot_general(x, wg_ref[0], nt, preferred_element_type=F32)
+        up_pre = lax.dot_general(x, wu_ref[0], nt, preferred_element_type=F32)
+        hidden_grad = lax.dot_general(g_ref[block, :], wd_ref[0], nt, preferred_element_type=F32)
+        lane = lax.broadcasted_iota(jnp.int32, (CORES * cap, LANES), 1)
+        scales = jnp.sum(
+            jnp.where(lane == ep, w_ref[block, :].astype(F32), 0.0), axis=1, keepdims=True
+        )
+        sigmoid = jax.nn.sigmoid(gate_pre)
+        activated = gate_pre * sigmoid
+        both = activated * up_pre
+        gate_part = jnp.sum(both * hidden_grad, axis=1, keepdims=True)
+        for who in range(CORES):
+            tile = jnp.broadcast_to(gate_part[who * cap : (who + 1) * cap], (cap, LANES))
+            tile = jnp.concatenate([tile, jnp.zeros((LANES - cap, LANES), F32)], axis=0).T
+            gates[0, core, pl.ds(q * CORES + who, 1), :] = tile[0:1]
+        weighted = scales * hidden_grad
+        gate_delta = (weighted * up_pre * sigmoid * (1.0 + gate_pre * (1.0 - sigmoid))).astype(BF16)
+        up_delta = (weighted * activated).astype(BF16)
+        hid_ref[block, :] = (scales * both).astype(BF16)
+        gd_ref[block, :] = gate_delta
+        ud_ref[block, :] = up_delta
+
+        @pl.loop(0, full // width)
+        def _(at):
+            columns = cols(at)
+            value = jnp.dot(gd_ref[block, :], wg_ref[0, :, columns], preferred_element_type=F32)
+            value += jnp.dot(ud_ref[block, :], wu_ref[0, :, columns], preferred_element_type=F32)
+            part_ref[block, columns] = value.astype(BF16)
+
+    def weight_grad(out_ref, delta_ref, rows_ref):
+        flipped = delta_ref[...].T
+
+        @pl.loop(0, full // half)
+        def _(at):
+            columns = pl.ds(pl.multiple_of(at * half, half), half)
+            out_ref[0, :, columns] = jnp.dot(
+                flipped, rows_ref[:, columns], preferred_element_type=F32
+            )
+
     pin_copies, one, two, back = {}, {}, {}, {}
-    pair_gate = send(gate_ref, gates.at[0, core], gate_sem.at[3], partner)
-    for k in order:
-        q = (z + k) % zs
+
+    def to_other_core(k):
         pin_copies[k] = send(
-            part_ref.at[rows(q, 1 - core)], pin.at[k], pin_sem.at[k], partner
+            part_ref.at[rows(source(k), 1 - core)], pin.at[k], pin_sem.at[k], partner
         )
+
+    def stage_one(k):
+        pin_copies[k].wait_recv()
+        comb[k] = (part_ref[rows(source(k)), :].astype(F32) + pin[k].astype(F32)).astype(BF16)
+        for which, near in enumerate((near_x, near_y)):
+            for i, at in ((1, diag), (0, near)):
+                one[k, which, i] = send(
+                    comb.at[k, :, half_cols(at, which)],
+                    first_in.at[k, which, i],
+                    one_sem.at[k, which, i],
+                    (ep, near),
+                )
+
+    def stage_two(k):
+        for which, far in enumerate((near_y, near_x)):
+            one[k, which, 1].wait_recv()
+            second_out[k, which] = (
+                comb[k, :, half_cols(far, which)].astype(F32) + first_in[k, which, 1].astype(F32)
+            ).astype(BF16)
+            two[k, which] = send(
+                second_out.at[k, which], second_in.at[k, which], two_sem.at[k, which], (ep, far)
+            )
+
+    def stage_three(k):
+        for which in range(2):
+            one[k, which, 0].wait_recv()
+            two[k, which].wait_recv()
+            final[k, :, which * half : (which + 1) * half] = (
+                comb[k, :, half_cols(tp, which)].astype(F32)
+                + first_in[k, which, 0].astype(F32)
+                + second_in[k, which].astype(F32)
+            ).astype(BF16)
+        if k:
+            back[k] = send(
+                final.at[k], back_ref.at[chip_rows(z)], back_sem.at[k],
+                (source(k) * CORES + core, tp),
+            )
+        else:
+            back_ref[chip_rows(z), :] = final[0]
+
+    for step in range(zs + 3):
+        for t in range(2):
+            if step < zs:
+                arrive(t, step) if (t, step) != (0, 0) else None
+            if 0 <= step - 1 < zs:
+                relay(t, step - 1)
+        if 0 <= step - 2 < zs:
+            last_part(step - 2)
+        k = step - 3
+        if k >= 0:
+            if k == 0:
+                for load in loads[3:]:
+                    load.wait()
+            compute(k)
+            to_other_core(k)
+            if k >= 1:
+                stage_one(k - 1)
+            if k >= 2:
+                stage_two(k - 2)
+            if k >= 3:
+                stage_three(k - 3)
+
+    last = zs - 1
+    pair_gate = send(gates.at[0, core], gates.at[0, core], gate_sem.at[3], partner)
+    stage_one(last)
+    if last >= 1:
+        stage_two(last - 1)
     pair_gate.wait_recv()
     gate_copies = [
         send(gates.at[0], gates.at[1 + i], gate_sem.at[i], (ep, to))
         for i, to in enumerate((near_x, near_y, diag))
     ]
-
-    def stage_one(k):
-        q = (z + k) % zs
-        pin_copies[k].wait_recv()
-        comb[k] = (part_ref[rows(q, core), :].astype(F32) + pin[k].astype(F32)).astype(BF16)
-        for which, near in enumerate((near_x, near_y)):
-            for i, at in enumerate((near, diag)):
-                one[k, which, i] = send(
-                    comb.at[k, :, cols(at, which)],
-                    first_in.at[k, which, i],
-                    one_sem.at[k, which, i],
-                    (ep, near),
-                )
-
-    def stage_two(k):
-        for which, far in enumerate((near_y, near_x)):
-            one[k, which, 1].wait_recv()
-            second_out[k, which] = (
-                comb[k, :, cols(far, which)].astype(F32) + first_in[k, which, 1].astype(F32)
-            ).astype(BF16)
-            two[k, which] = send(
-                second_out.at[k, which], second_in.at[k, which], two_sem.at[k, which], (ep, far)
-            )
-
-    def stage_three(k):
-        q = (z + k) % zs
-        for which in range(2):
-            one[k, which, 0].wait_recv()
-            two[k, which].wait_recv()
-            final[k, :, which * half : (which + 1) * half] = (
-                comb[k, :, cols(tp, which)].astype(F32)
-                + first_in[k, which, 0].astype(F32)
-                + second_in[k, which].astype(F32)
-            ).astype(BF16)
-        if k:
-            back[k] = send(
-                final.at[k], back_ref.at[chip_rows(z)], z_sem.at[k], (q * CORES + core, tp)
-            )
-        else:
-            back_ref[chip_rows(z), :] = final[0]
-
-    for k in order:
-        stage_one(k)
+    weight_grad(dwd_ref, hid_ref, g_ref)
+    stage_two(last)
+    for k in range(max(last - 2, 0), last):
+        stage_three(k)
     for copy in gate_copies:
         copy.wait_recv()
     total_ref[z] = gates[0] + gates[1] + gates[2] + gates[3]
@@ -264,11 +326,9 @@
         send(total_ref.at[z], total_ref.at[z], gz_sem.at[k], (((z + k) % zs) * CORES + core, tp))
         for k in range(1, zs)
     ]
-    for at, k in enumerate(order):
-        stage_two(k)
-        if at:
-            stage_three(order[at - 1])
-    stage_three(order[-1])
+    weight_grad(dwg_ref, gd_ref, x_ref)
+    stage_three(last)
+    weight_grad(dwu_ref, ud_ref, x_ref)
     for copy in list(back.values()) + gate_back:
         copy.wait_recv()
     send.finish()
@@ -424,74 +484,42 @@
     chosen = expert_ids[:, :, None] == jnp.arange(LANES, dtype=jnp.int32)
     wmat = jnp.sum(jnp.where(chosen, gate_weights[:, :, None].astype(F32), 0.0), axis=1).astype(BF16)
 
+    half = width // 2
+    hidden = gate_w.shape[1]
     n_send = 3 + 3 * (zs - 1) + zs + 2 * zs * 7
-    inputs, cotangent, weights = pl.pallas_call(
-        functools.partial(dispatch_kernel, zs, cap, width),
+    n_send += 4 + zs + 4 * zs + 2 * zs + 2 * (zs - 1)
+    dw_shape = jax.ShapeDtypeStruct(gate_w.shape, F32)
+    any_spec = pl.BlockSpec(memory_space=pl.ANY)
+    sem = pltpu.SemaphoreType.DMA
+    back, totals, gate_grad_w, up_grad_w, down_grad = pl.pallas_call(
+        functools.partial(route_kernel, zs, cap, width),
         out_shape=(
-            jax.ShapeDtypeStruct((slots, full_width), BF16),
-            jax.ShapeDtypeStruct((slots, full_width), BF16),
-            jax.ShapeDtypeStruct((slots, LANES), BF16),
+            jax.ShapeDtypeStruct((zs * cap, width), BF16),
+            jax.ShapeDtypeStruct((zs, CORES, ep_count, LANES), F32),
+            dw_shape,
+            dw_shape,
+            dw_shape,
         ),
-        in_specs=[VMEM_SPEC] * 6,
-        out_specs=(VMEM_SPEC,) * 3,
+        in_specs=[any_spec] * 3 + [VMEM_SPEC] * 3 + [any_spec] * 3,
+        out_specs=(VMEM_SPEC,) * 5,
         scratch_shapes=[
+            pltpu.VMEM((tok_count, width), BF16),
+            pltpu.VMEM((tok_count, width), BF16),
+            pltpu.VMEM((tok_count, width), BF16),
+            pltpu.VMEM(gate_w.shape, BF16),
+            pltpu.VMEM(gate_w.shape, BF16),
+            pltpu.VMEM(gate_w.shape, BF16),
+            pltpu.VMEM((slots, full_width), BF16),
+            pltpu.VMEM((slots, full_width), BF16),
+            pltpu.VMEM((slots, LANES), BF16),
             pltpu.VMEM((zs * cap, width), BF16),
             pltpu.VMEM((zs * cap, width), BF16),
             pltpu.VMEM((zs * cap, LANES), BF16),
             pltpu.VMEM((4, 8, -(-tok_count // LANES) * LANES), F32),
-            pltpu.SemaphoreType.DMA((n_send,)),
-            pltpu.SemaphoreType.DMA((3,)),
-            pltpu.SemaphoreType.DMA((2, zs)),
-            pltpu.SemaphoreType.DMA((zs,)),
-            pltpu.SemaphoreType.DMA((zs,)),
-            pltpu.SemaphoreType.DMA((2, zs, 3)),
-            pltpu.SemaphoreType.DMA((2, zs, 4)),
-        ],
-        compiler_params=pltpu.CompilerParams(
-            collective_id=0, has_side_effects=True, vmem_limit_bytes=48 * 1024 * 1024
-        ),
-    )(tokens, moe_out, out_grad, norm_gain.reshape(1, width), perm, wmat)
-
-    core = lax.axis_index("ep")
-    lane = jnp.arange(LANES, dtype=jnp.int32)
-    scales = jnp.sum(
-        jnp.where(lane == core, weights.astype(F32), 0.0), axis=1, keepdims=True
-    )
-    w_gate, w_up, w_down = gate_w[0], up_w[0], down_w[0]
-
-    def contract(a, b, dims):
-        return lax.dot_general(a, b, (dims, ((), ())), preferred_element_type=F32)
-
-    gate_pre = contract(inputs, w_gate, ((1,), (1,)))
-    up_pre = contract(inputs, w_up, ((1,), (1,)))
-    hidden_grad = contract(cotangent, w_down, ((1,), (1,)))
-    sigmoid = jax.nn.sigmoid(gate_pre)
-    activated = gate_pre * sigmoid
-    gate_part = jnp.sum(activated * up_pre * hidden_grad, axis=1).reshape(ep_count, cap)
-    gate_part = jnp.pad(gate_part, ((0, 0), (0, LANES - cap)))
-    scaled_hidden = (scales * activated * up_pre).astype(BF16)
-    gate_delta = (
-        scales * hidden_grad * up_pre * sigmoid * (1.0 + gate_pre * (1.0 - sigmoid))
-    ).astype(BF16)
-    up_delta = (scales * hidden_grad * activated).astype(BF16)
-    partial_value = (
-        contract(gate_delta, w_gate, ((1,), (0,))) + contract(up_delta, w_up, ((1,), (0,)))
-    ).astype(BF16)
-    down_grad = contract(scaled_hidden, cotangent, ((0,), (0,)))[None]
-    gate_grad_w = contract(gate_delta, inputs, ((0,), (0,)))[None]
-    up_grad_w = contract(up_delta, inputs, ((0,), (0,)))[None]
-
-    half = width // 2
-    n_send = 4 + zs + 4 * zs + 2 * zs + 2 * (zs - 1)
-    back, totals = pl.pallas_call(
-        functools.partial(return_kernel, zs, cap, width),
-        out_shape=(
-            jax.ShapeDtypeStruct((zs * cap, width), BF16),
-            jax.ShapeDtypeStruct((zs, CORES, ep_count, LANES), F32),
-        ),
-        in_specs=[VMEM_SPEC] * 2,
-        out_specs=(VMEM_SPEC,) * 2,
-        scratch_shapes=[
+            pltpu.VMEM((slots, hidden), BF16),
+            pltpu.VMEM((slots, hidden), BF16),
+            pltpu.VMEM((slots, hidden), BF16),
+            pltpu.VMEM((slots, full_width), BF16),
             pltpu.VMEM((zs, cap, full_width), BF16),
             pltpu.VMEM((zs, cap, full_width), BF16),
             pltpu.VMEM((zs, 2, 2, cap, half), BF16),
@@ -499,20 +527,31 @@
             pltpu.VMEM((zs, 2, cap, half), BF16),
             pltpu.VMEM((zs, cap, width), BF16),
             pltpu.VMEM((4, CORES, ep_count, LANES), F32),
-            pltpu.SemaphoreType.DMA((n_send,)),
-            pltpu.SemaphoreType.DMA((zs,)),
-            pltpu.SemaphoreType.DMA((zs, 2, 2)),
-            pltpu.SemaphoreType.DMA((zs, 2)),
-            pltpu.SemaphoreType.DMA((zs,)),
-            pltpu.SemaphoreType.DMA((4,)),
-            pltpu.SemaphoreType.DMA((zs,)),
+            sem((6,)),
+            sem((n_send,)),
+            sem((3,)),
+            sem((2, zs)),
+            sem((zs,)),
+            sem((zs,)),
+            sem((2, zs, 3)),
+            sem((2, zs, 4)),
+            sem((zs,)),
+            sem((zs, 2, 2)),
+            sem((zs, 2)),
+            sem((zs,)),
+            sem((4,)),
+            sem((zs,)),
         ],
         compiler_params=pltpu.CompilerParams(
-            collective_id=1, has_side_effects=True, vmem_limit_bytes=48 * 1024 * 1024
+            collective_id=0, has_side_effects=True, vmem_limit_bytes=60 * 1024 * 1024
         ),
-    )(partial_value, gate_part)
-
-    token_grad = contract(perm, back, ((0,), (0,))).astype(BF16)
+    )(
+        tokens, moe_out, out_grad, norm_gain.reshape(1, width), perm, wmat, gate_w, up_w, down_w
+    )
+
+    token_grad = lax.dot_general(
+        perm, back, (((0,), (0,)), ((), ())), preferred_element_type=F32
+    ).astype(BF16)
     me = lax.axis_index("ep")
     mine = lax.dynamic_index_in_dim(totals, me, 2, keepdims=False)[:, :, :cap]
     mine = mine.astype(BF16).astype(F32)

time: 114 us -> 92.6 us (0.81)
  matrix products: 30.3 us -> 2.14 us
  local copies, waits for them, and re-layouts: 5.79 us -> 9.63 us
  Pallas kernels: 73.2 us -> 74.9 us
    dot_general x9 -> x1, matrix products: 30.1 us -> 1.99 us  [local(): lax.dot_general(perm, back, (((0,), (0,)), ((), ())), preferred_element_t...]
    unnamed x25 -> x8, local copies, waits for them, and re-layouts: 5.59 us -> 8.75 us
    pallas_call x2 -> x1, Pallas kernels: 73.2 us -> 74.9 us  [local(): pl.pallas_call(functools.partial(route_kernel, zs, cap, width), out_shape...]
where the time goes in v2:
time: 92.6 us; the launch traced here: 92.2 us
  Pallas kernels  74.9 us (81%)
  local copies, waits for them, and re-layouts  9.63 us (10%)
  other arithmetic  4.88 us (5%)
  matrix products  2.14 us (2%)
    pallas_call x1, Pallas kernels, local(): pl.pallas_call(functools.partial(route_kernel, zs, cap, width), out_shape...  74.9 us
    unnamed x8, local copies, waits for them, and re-layouts  8.75 us
    dot_general x1, matrix products, local(): lax.dot_general(perm, back, (((0,), (0,)), ((), ())), preferred_element_t...  1.99 us

profile of v2, /device:TPU:0, one launch (start us, length us, event | category | flops | bytes accessed | tf_op | source)
XLA Modules:
  0.0 92.2 jit_solution(8062081085184204972)
XLA Ops:
  0.6 0.7 convert_element_type.28
  1.3 0.1 eq.88
  1.4 0.7 and_select_fusion
  2.2 0.1 fusion
  2.3 1.5 %select_reduce_fusion.2.wmat_ref = bf16[192,128]{1,0:T(8,128)(2,1)} fusion(f32[192,2]{0,1:T(2,128)S(1)} %convert_element_type.28, s32[192,2]{0,1:T(2,128)} %param.14), kind=kLoop, calls=%fused_computation.9 | loop fusion | flops 122880 | bytes 52224 | tf_op jit(solution)/shard_map/reduce_sum | solution.py:485
  3.8 0.8 fusion.3
  4.6 74.9 %shard_map.128 = (bf16[384,512]{1,0:T(8,128)(2,1)}, f32[4,2,8,128]{3,2,1,0:T(8,128)}, f32[1,384,2048]{2,1,0:T(8,128)}, f32[1,384,2048]{2,1,0:T(8,128)}, f32[1,384,2048]{2,1,0:T(8,128)}) custom-call(bf16[192,2048]{1,0:T(8,128)(2,1)} %tok_hbm.1, bf16[192,512]{1,0:T(8,128)(2,1)} %moe_hbm.1, bf16[192,512]{1,0:T(8,128)(2,1)} %grad_hbm.1, f32[1,512]{1,0:T(1,128)} %bitcast.22, ...), custom_call_target="tpu_custom_call" | custom-call | tf_op jit(solution)/shard_map/pallas_call | solution.py:494
  79.5 2.0 %convolution_convert_fusion = bf16[192,512]{1,0:T(8,128)(2,1)} fusion(pred[384,192]{1,0:T(32,128)(4,1)S(1)} %get-tuple-element.22, bf16[384,512]{1,0:T(8,128)(2,1)} %get-tuple-element.10), kind=kOutput, calls=%fused_computation | convolution fusion | flops 75595776 | bytes 663552 | tf_op jit(solution)/shard_map/dot_general | solution.py:552
  81.5 0.8 dynamic-slice_convert_fusion
  82.3 0.6 select_reduce_fusion.1
  82.9 0.6 pad_maximum_fusion
  83.5 0.0 copy-start.1
  83.5 4.1 %copy.31 = f32[1,384,2048]{2,1,0:T(8,128)} copy(f32[1,384,2048]{2,1,0:T(8,128)} %get-tuple-element.36) | data formatting | bytes 6291456
  87.5 0.0 copy-done.1
  87.5 0.0 copy-start
  87.5 1.7 %copy.32 = f32[1,384,2048]{2,1,0:T(8,128)} copy(f32[1,384,2048]{2,1,0:T(8,128)S(1)} %copy-done.1) | data formatting | bytes 6291456
  89.2 1.4 %copy-done = f32[1,384,2048]{2,1,0:T(8,128)S(1)} copy-done((f32[1,384,2048]{2,1,0:T(8,128)S(1)}, f32[1,384,2048]{2,1,0:T(8,128)}, u32[]{:S(2)}) %copy-start) | copy-done | bytes 3145752
  90.6 1.7 %copy.33 = f32[1,384,2048]{2,1,0:T(8,128)} copy(f32[1,384,2048]{2,1,0:T(8,128)S(1)} %copy-done) | data formatting | bytes 6291456
  (9 shorter events, 0.1 us)
Async XLA Ops:
  83.5 4.1 %copy-start.1 = (f32[1,384,2048]{2,1,0:T(8,128)S(1)}, f32[1,384,2048]{2,1,0:T(8,128)}, u32[]{:S(2)}) copy-start(f32[1,384,2048]{2,1,0:T(8,128)} %get-tuple-element.37) | copy-start | bytes 9437188
  87.5 3.0 %copy-start = (f32[1,384,2048]{2,1,0:T(8,128)S(1)}, f32[1,384,2048]{2,1,0:T(8,128)}, u32[]{:S(2)}) copy-start(f32[1,384,2048]{2,1,0:T(8,128)} %get-tuple-element.38) | copy-start | bytes 9437188

commit v3 on v2

--- a/solution.py
+++ b/solution.py
@@ -220,6 +220,9 @@
         gd_ref[block, :] = gate_delta
         ud_ref[block, :] = up_delta
 
+    def input_grad(k):
+        block = pl.ds(pl.multiple_of(source(k) * (CORES * cap), 16), CORES * cap)
+
         @pl.loop(0, full // width)
         def _(at):
             columns = cols(at)
@@ -283,42 +286,42 @@
         else:
             back_ref[chip_rows(z), :] = final[0]
 
-    for step in range(zs + 3):
+    last = zs - 1
+    for step in range(zs + 2):
+        if 0 <= step - 2:
+            last_part(step - 2)
         for t in range(2):
             if step < zs:
                 arrive(t, step) if (t, step) != (0, 0) else None
             if 0 <= step - 1 < zs:
                 relay(t, step - 1)
-        if 0 <= step - 2 < zs:
-            last_part(step - 2)
-        k = step - 3
+        k = step - 2
         if k >= 0:
             if k == 0:
                 for load in loads[3:]:
                     load.wait()
             compute(k)
-            to_other_core(k)
             if k >= 1:
                 stage_one(k - 1)
             if k >= 2:
-                stage_two(k - 2)
-            if k >= 3:
-                stage_three(k - 3)
-
-    last = zs - 1
+                stage_three(k - 2)
+            input_grad(k)
+            to_other_core(k)
+            if k >= 1:
+                stage_two(k - 1)
+
     pair_gate = send(gates.at[0, core], gates.at[0, core], gate_sem.at[3], partner)
+    weight_grad(dwd_ref, hid_ref, g_ref)
     stage_one(last)
     if last >= 1:
-        stage_two(last - 1)
+        stage_three(last - 1)
     pair_gate.wait_recv()
     gate_copies = [
         send(gates.at[0], gates.at[1 + i], gate_sem.at[i], (ep, to))
         for i, to in enumerate((near_x, near_y, diag))
     ]
-    weight_grad(dwd_ref, hid_ref, g_ref)
+    weight_grad(dwg_ref, gd_ref, x_ref)
     stage_two(last)
-    for k in range(max(last - 2, 0), last):
-        stage_three(k)
     for copy in gate_copies:
         copy.wait_recv()
     total_ref[z] = gates[0] + gates[1] + gates[2] + gates[3]
@@ -326,9 +329,8 @@
         send(total_ref.at[z], total_ref.at[z], gz_sem.at[k], (((z + k) % zs) * CORES + core, tp))
         for k in range(1, zs)
     ]
-    weight_grad(dwg_ref, gd_ref, x_ref)
+    weight_grad(dwu_ref, ud_ref, x_ref)
     stage_three(last)
-    weight_grad(dwu_ref, ud_ref, x_ref)
     for copy in list(back.values()) + gate_back:
         copy.wait_recv()
     send.finish()
@@ -489,7 +491,7 @@
     n_send = 3 + 3 * (zs - 1) + zs + 2 * zs * 7
     n_send += 4 + zs + 4 * zs + 2 * zs + 2 * (zs - 1)
     dw_shape = jax.ShapeDtypeStruct(gate_w.shape, F32)
-    any_spec = pl.BlockSpec(memory_space=pl.ANY)
+    any_spec = pl.BlockSpec(memory_space=pltpu.HBM)
     sem = pltpu.SemaphoreType.DMA
     back, totals, gate_grad_w, up_grad_w, down_grad = pl.pallas_call(
         functools.partial(route_kernel, zs, cap, width),
@@ -543,10 +545,14 @@
             sem((zs,)),
         ],
         compiler_params=pltpu.CompilerParams(
-            collective_id=0, has_side_effects=True, vmem_limit_bytes=60 * 1024 * 1024
+            collective_id=0, has_side_effects=True, vmem_limit_bytes=36 * 1024 * 1024
         ),
     )(
-        tokens, moe_out, out_grad, norm_gain.reshape(1, width), perm, wmat, gate_w, up_w, down_w
+        *(pltpu.with_memory_space_constraint(a, pltpu.HBM) for a in (tokens, moe_out, out_grad)),
+        norm_gain.reshape(1, width),
+        perm,
+        wmat,
+        *(pltpu.with_memory_space_constraint(a, pltpu.HBM) for a in (gate_w, up_w, down_w)),
     )
 
     token_grad = lax.dot_general(

time: 92.6 us -> 84.3 us (0.910)
  local copies, waits for them, and re-layouts: 9.63 us -> 5.79 us
  Pallas kernels: 74.9 us -> 72.6 us
  other arithmetic: 4.88 us -> 3.56 us
  matrix products: 2.14 us -> 1.15 us
    unnamed x8 -> x6, local copies, waits for them, and re-layouts: 8.75 us -> 5.67 us
    pallas_call x1, Pallas kernels: 74.9 us -> 72.6 us  [local(): pl.pallas_call(functools.partial(route_kernel, zs, cap, width), out_shape...]
    dot_general x1, matrix products: 1.99 us -> 1 us  [local(): lax.dot_general(perm, back, (((0,), (0,)), ((), ())), preferred_element_t...]
where the time goes in v3:
time: 84.3 us; the launch traced here: 83.8 us
  Pallas kernels  72.6 us (86%)
  local copies, waits for them, and re-layouts  5.79 us (7%)
  other arithmetic  3.56 us (4%)
  matrix products  1.15 us (1%)
    pallas_call x1, Pallas kernels, local(): pl.pallas_call(functools.partial(route_kernel, zs, cap, width), out_shape...  72.6 us
    unnamed x6, local copies, waits for them, and re-layouts  5.67 us

profile of v3, /device:TPU:0, one launch (start us, length us, event | category | flops | bytes accessed | tf_op | source)
XLA Modules:
  0.0 83.8 jit_solution(7169332109846630839)
XLA Ops:
  0.6 0.7 convert_element_type.28
  1.3 0.1 eq.88
  1.4 0.7 and_select_fusion
  2.2 0.1 fusion
  2.3 0.9 %select_reduce_fusion.2.wmat_ref = bf16[192,128]{1,0:T(8,128)(2,1)S(1)} fusion(f32[192,2]{0,1:T(2,128)S(1)} %convert_element_type.28, s32[192,2]{0,1:T(2,128)} %param.14), kind=kLoop, calls=%fused_computation.9 | loop fusion | flops 122880 | bytes 52224 | tf_op jit(solution)/shard_map/reduce_sum | solution.py:487
  3.2 0.1 fusion.3
  3.3 0.0 copy-start
  3.3 0.7 copy-done
  4.0 72.6 %shard_map.128 = (bf16[384,512]{1,0:T(8,128)(2,1)S(1)}, f32[4,2,8,128]{3,2,1,0:T(8,128)S(1)}, f32[1,384,2048]{2,1,0:T(8,128)S(1)}, f32[1,384,2048]{2,1,0:T(8,128)S(1)}, f32[1,384,2048]{2,1,0:T(8,128)S(1)}) custom-call(bf16[192,2048]{1,0:T(8,128)(2,1)} %tok_hbm.1, bf16[192,512]{1,0:T(8,128)(2,1)} %moe_hbm.1, bf16[192,512]{1,0:T(8,128)(2,1)} %grad_hbm.1, ...), custom_call_target="tpu_custom_call" | custom-call | tf_op jit(solution)/shard_map/pallas_call | solution.py:496
  76.6 1.0 %convolution_convert_fusion = bf16[192,512]{1,0:T(8,128)(2,1)} fusion(pred[384,192]{1,0:T(32,128)(4,1)S(1)} %get-tuple-element.22, bf16[384,512]{1,0:T(8,128)(2,1)S(1)} %get-tuple-element.10), kind=kOutput, calls=%fused_computation | convolution fusion | flops 75595776 | bytes 663552 | tf_op jit(solution)/shard_map/dot_general | solution.py:558
  77.7 0.6 select_reduce_fusion.1
  78.3 0.6 pad_maximum_fusion
  78.8 1.7 %copy.31 = f32[1,384,2048]{2,1,0:T(8,128)} copy(f32[1,384,2048]{2,1,0:T(8,128)S(1)} %get-tuple-element.36) | data formatting | bytes 6291456
  80.5 1.7 %copy.32 = f32[1,384,2048]{2,1,0:T(8,128)} copy(f32[1,384,2048]{2,1,0:T(8,128)S(1)} %get-tuple-element.37) | data formatting | bytes 6291456
  82.2 1.7 %copy.33 = f32[1,384,2048]{2,1,0:T(8,128)} copy(f32[1,384,2048]{2,1,0:T(8,128)S(1)} %get-tuple-element.38) | data formatting | bytes 6291456
  (10 shorter events, 0.1 us)
Async XLA Ops:
  3.3 0.7 copy-start
